TPU v7x, 32 devices: a whole 2x2x4 slice. The times are simulated.
32 devices in a mesh: kv: 8 (over z, y), tp: 4 (over x, core).
Axes of the slice: x: 2, y: 2, z: 4, core: 2. Of those that a mesh axis runs over, the one named last changes fastest.
Arguments:
- hidden_rows: bfloat16 [128, 4096], P('kv', 'tp'), may hold values from -16 to 16
- carried_state: float32 [128, 524288], P('kv', 'tp'), may hold values from -6 to 6
- norm_gain: bfloat16 [4096], replicated, may hold values from 0.099609375 to 1.8984375
- w_query: bfloat16 [4096, 2048], P('kv', 'tp'), may hold values from -0.09375 to 0.09375
- w_key: bfloat16 [4096, 2048], P('kv', 'tp'), may hold values from -0.09375 to 0.09375
- w_decay: bfloat16 [4096, 2048], P('kv', 'tp'), may hold values from -0.375 to 0.375
- w_value: bfloat16 [4096, 4096], P('kv', 'tp'), may hold values from -0.09375 to 0.09375
- w_gate: bfloat16 [4096, 4096], P('kv', 'tp'), may hold values from -0.09375 to 0.09375
- decay_bias: float32 [2048], P('tp'), may hold values from -32 to 8
- head_gain: bfloat16 [256], replicated, may hold values from 0.099609375 to 1.8984375
- w_out: bfloat16 [4096, 4096], P('tp', 'kv'), may hold values from -0.09375 to 0.09375
- mlp_gain: bfloat16 [4096], P('tp'), may hold values from 0.099609375 to 1.8984375
- w_up: bfloat16 [4096, 16384], P('tp', 'kv'), may hold values from -0.09375 to 0.09375
- w_down: bfloat16 [16384, 4096], P('kv', 'tp'), may hold values from -0.046875 to 0.046875
Outputs:
- updated_rows: bfloat16 [128, 4096], P('kv', 'tp')
- new_state: float32 [128, 524288], P('kv', 'tp')
All inputs are finite; a program needn't handle non-finite values.
Results may differ from a plain program's by a relative error of at most 0.025.
Values may be sent and summed in bfloat16 or wider, within the bound.
A program may use at most 128 MiB of HBM per device.

v0:
```python
import jax
import jax.numpy as jnp
from jax import lax
from jax.sharding import PartitionSpec as P

D = 4096
DK = 128
DV = 256
epsilon = 1e-06
decay_normalizer = 16.0


def body(
    hidden_rows,
    carried_state,
    norm_gain,
    w_query,
    w_key,
    w_decay,
    w_value,
    w_gate,
    decay_bias,
    head_gain,
    w_out,
    mlp_gain,
    w_up,
    w_down,
):
    seq_rows = hidden_rows.shape[0]
    heads_here = decay_bias.shape[0] // DK
    gathered = lax.all_gather(hidden_rows, "tp", axis=1, tiled=True)
    whole_inputs = gathered.astype(jnp.float32)
    normed = (
        whole_inputs
        * lax.rsqrt(jnp.mean(whole_inputs * whole_inputs, axis=-1, keepdims=True) + epsilon)
        * norm_gain.astype(jnp.float32)
    ).astype(jnp.bfloat16)
    weights = (w_query, w_key, w_decay, w_value, w_gate)
    feature_blocks = lax.all_to_all(normed, "kv", split_axis=1, concat_axis=0, tiled=True)
    joined = jnp.concatenate(weights, axis=1)
    block_rows = feature_blocks
    summed = lax.psum_scatter(
        jnp.dot(block_rows, joined, preferred_element_type=jnp.float32).astype(jnp.bfloat16),
        "kv",
        scatter_dimension=0,
        tiled=True,
    ).astype(jnp.float32)
    projected = []
    offset = 0
    for weight in weights:
        projected.append(summed[:, offset : offset + weight.shape[1]])
        offset = offset + weight.shape[1]
    queries, keys_new, decay_pre, values, out_gate = [
        item.astype(jnp.bfloat16) for item in projected
    ]
    log_decay = jax.nn.log_sigmoid(decay_pre.astype(jnp.float32) + decay_bias) / decay_normalizer
    log_decay = log_decay.reshape(seq_rows, heads_here, DK)
    carried = carried_state.reshape(seq_rows, heads_here, DK, DV)
    key_heads = keys_new.astype(jnp.float32).reshape(seq_rows, heads_here, DK)
    value_heads = values.astype(jnp.float32).reshape(seq_rows, heads_here, DV)
    new_state = (
        jnp.exp(log_decay)[..., None] * carried + key_heads[..., None] * value_heads[..., None, :]
    )
    query_heads = queries.astype(jnp.float32).reshape(seq_rows, heads_here, DK) * DK ** (-0.5)
    head_out = jnp.einsum("bhk,bhkv->bhv", query_heads, new_state, precision=lax.Precision.HIGHEST)
    gate_heads = out_gate.astype(jnp.float32).reshape(seq_rows, heads_here, DV)
    mixed = head_out * lax.rsqrt(jnp.mean(head_out * head_out, axis=-1, keepdims=True) + epsilon)
    mixed = (mixed * head_gain.astype(jnp.float32) * jax.nn.silu(gate_heads)).astype(jnp.bfloat16)
    mixed = mixed.reshape(seq_rows, heads_here * DV)
    partial_out = jnp.dot(
        mixed, lax.all_gather(w_out, "kv", axis=1, tiled=True), preferred_element_type=jnp.float32
    ).astype(jnp.bfloat16)
    attn_out = lax.psum_scatter(
        partial_out.astype(jnp.float32).astype(jnp.bfloat16), "tp", scatter_dimension=1, tiled=True
    )
    residual = (hidden_rows.astype(jnp.float32) + attn_out.astype(jnp.float32)).astype(jnp.bfloat16)
    resid_float = residual.astype(jnp.float32)
    total_squares = lax.psum(jnp.sum(resid_float * resid_float, axis=-1), "tp")
    row_scale = lax.rsqrt(total_squares / D + epsilon)
    mlp_input = (resid_float * row_scale[:, None] * mlp_gain.astype(jnp.float32)).astype(
        jnp.bfloat16
    )
    up_partial = jnp.dot(
        lax.all_gather(mlp_input, "kv", axis=0, tiled=True),
        w_up,
        preferred_element_type=jnp.float32,
    ).astype(jnp.bfloat16)
    up_sum = lax.psum(up_partial.astype(jnp.float32).astype(jnp.bfloat16), "tp").astype(jnp.float32)
    activation = jnp.square(jax.nn.relu(up_sum)).astype(jnp.bfloat16)
    block_rows = activation
    mlp_total = lax.psum_scatter(
        jnp.dot(block_rows, w_down, preferred_element_type=jnp.float32).astype(jnp.bfloat16),
        "kv",
        scatter_dimension=0,
        tiled=True,
    )
    updated_rows = (resid_float + mlp_total.astype(jnp.float32)).astype(jnp.bfloat16)
    return (updated_rows, new_state.reshape(seq_rows, heads_here * DK * DV))


def solution(mesh):
    return jax.shard_map(
        body,
        mesh=mesh,
        in_specs=(
            P("kv", "tp"),
            P("kv", "tp"),
            P(),
            P("kv", "tp"),
            P("kv", "tp"),
            P("kv", "tp"),
            P("kv", "tp"),
            P("kv", "tp"),
            P("tp"),
            P(),
            P("tp", "kv"),
            P("tp"),
            P("tp", "kv"),
            P("kv", "tp"),
        ),
        out_specs=(P("kv", "tp"), P("kv", "tp")),
        check_vma=False,
    )
```

profile of v0, /device:TPU:0, one launch (start us, length us, event | category | flops | bytes accessed | tf_op | source)
XLA Modules:
  0.0 400.0 jit_solution(15394609910348088016)
XLA Ops:
  7.2 6.7 %all_gather.9 = bf16[16,4096]{1,0:T(8,128)(2,1)S(1)} all-gather(bf16[16,1024]{1,0:T(8,128)(2,1)} %param.14), channel_id=1, replica_groups=mesh['kv'=8,'tp'=4] {'tp'}, dimensions={1}, use_global_device_ids=true | all-gather | bytes 163840 | tf_op jit(solution)/shard_map/all_gather | solution.py:31
  13.9 0.1 fusion.5
  14.0 0.7 convert_element_type.78
  14.7 0.1 fusion.7
  14.8 0.7 copy.28
  15.5 6.2 %all-to-all-start = ((bf16[16,8,512]{2,0,1:T(8,128)(2,1)}), bf16[16,8,512]{2,0,1:T(8,128)(2,1)S(1)}, u32[]{:S(2)}, u32[]{:S(2)}) async-start(bf16[16,8,512]{2,0,1:T(8,128)(2,1)} %bitcast.37), calls=%async_computation | async-start | bytes 262144 | tf_op jit(solution)/shard_map/all_to_all | solution.py:39
  21.7 0.0 reduce-scatter.4.cloned.1.call-start
  21.8 1.9 constant_dynamic-update-slice_fusion.4
  23.6 1.9 constant_dynamic-update-slice_fusion.3
  25.5 1.9 constant_dynamic-update-slice_fusion.2
  27.4 2.3 constant_dynamic-update-slice_fusion.1
  29.6 2.3 constant_dynamic-update-slice_fusion
  31.9 0.0 all-to-all-done
  31.9 3.7 convolution_convert_fusion
  35.6 0.0 reduce-scatter.4.cloned.1.call-update
  35.6 0.0 all-gather.2.cloned.1.call-start
  35.7 0.7 all-gather.2.cloned.1.call-update
  36.4 0.0 reduce-scatter.6.cloned.1.call-start
  36.4 0.0 copy-start.4
  36.4 0.0 copy-start.2
  36.5 9.3 %copy.21 = f32[2,8,512,256]{3,2,1,0:T(8,128)} copy(f32[2,8,512,256]{3,1,2,0:T(8,128)} %bitcast.41) | data formatting | bytes 16777216
  45.7 0.0 copy-done.4
  45.7 55.1 %reduce-scatter.4.cloned.1.call-done = bf16[16,3584]{1,0:T(8,128)(2,1)} async-done(((bf16[128,3584]{1,0:T(8,128)(2,1)}), bf16[16,3584]{1,0:T(8,128)(2,1)}) %reduce-scatter.4.cloned.1.call-update) | async-done | bytes 114704 | tf_op jit(solution)/shard_map/reduce_scatter | solution.py:42
  100.8 0.8 slice_convert_fusion.1
  101.6 0.0 copy-done.2
  101.6 0.8 fusion.18
  102.5 0.7 slice_convert_fusion.2
  103.2 7.5 %fusion = f32[16,4,1,256]{3,2,1,0:T(1,128)S(1)} fusion(f32[16,4,128,1]{2,3,1,0:T(1,128)S(1)} %bitcast.47, f32[16,4,128,256]{3,2,1,0:T(8,128)} %bitcast.38, f32[16,4,128]{2,1,0:T(4,128)S(1)} %exp.21, f32[16,4,256]{2,1,0:T(4,128)S(1)} %reshape.62, f32[16,4,128]{2,1,0:T(4,128)S(1)} %reshape.61), kind=kOutput, calls=%fused_computation.1 | convolution fusion | flops 31457280 | bytes 8617984 | tf_op jit(solution)/shard_map/bhk,bhkv->bhv/dot_general | solution.py:65
  110.8 0.0 copy-start.3
  110.8 0.0 copy-start
  110.8 0.1 fusion.13
  110.9 0.1 fusion.15
  111.0 115.8 %all-gather.2.cloned.1.call-done = bf16[1024,4096]{1,0:T(8,128)(2,1)} async-done(((bf16[1024,512]{1,0:T(8,128)(2,1)}), bf16[1024,4096]{1,0:T(8,128)(2,1)}) %all-gather.2.cloned.1.call-update) | async-done | bytes 8388624 | tf_op jit(solution)/shard_map/all_gather | solution.py:71
  226.8 5.2 %convolution_convert_fusion.1 = bf16[16,4096]{1,0:T(8,128)(2,1)} fusion(bf16[16,1024]{1,0:T(8,128)(2,1)S(1)} %bitcast.46, bf16[1024,4096]{1,0:T(8,128)(2,1)} %all-gather.2.cloned.1.call-done), kind=kOutput, calls=%fused_computation.5 | convolution fusion | flops 134283264 | bytes 8552448 | tf_op jit(solution)/shard_map/dot_general | solution.py:70
  232.1 0.0 reduce-scatter.6.cloned.1.call-update
  232.1 0.0 all-reduce.2.cloned.1.call-start
  232.1 0.0 copy-done.3
  232.2 17.9 %reduce-scatter.6.cloned.1.call-done = bf16[16,1024]{1,0:T(8,128)(2,1)} async-done(((bf16[16,4096]{1,0:T(8,128)(2,1)}), bf16[16,1024]{1,0:T(8,128)(2,1)}) %reduce-scatter.6.cloned.1.call-update) | async-done | bytes 32784 | tf_op jit(solution)/shard_map/reduce_scatter | solution.py:73
  250.1 0.0 copy-done
  250.1 0.9 fusion.9
  250.9 5.8 %psum.14 = f32[16]{0:T(128)S(1)} all-reduce(f32[16]{0:T(128)S(1)} %fusion.9), channel_id=1, replica_groups=mesh['kv'=8,'tp'=4] {'tp'}, use_global_device_ids=true, to_apply=%region_5.6 | all-reduce | flops 16 | bytes 128 | tf_op jit(solution)/shard_map/psum | solution.py:78
  256.7 0.8 fusion.11
  257.5 31.1 %all_gather.11 = bf16[128,1024]{1,0:T(8,128)(2,1)S(1)} all-gather(bf16[16,1024]{1,0:T(8,128)(2,1)S(1)} %fusion.11), channel_id=1, replica_groups=mesh['kv'=8,'tp'=4] {'kv'}, dimensions={0}, use_global_device_ids=true | all-gather | bytes 294912 | tf_op jit(solution)/shard_map/all_gather | solution.py:84
  288.6 3.8 convolution_convert_fusion.2
  292.4 0.0 all-reduce.2.cloned.1.call-update
  292.5 0.2 reduce-scatter.8.cloned.1.call-start
  292.7 1.3 broadcast_multiply_fusion
  294.0 8.3 %copy.24 = f32[2,8,512,256]{3,1,2,0:T(8,128)} copy(f32[2,8,512,256]{3,2,1,0:T(8,128)S(1)} %bitcast.39) | data formatting | bytes 16777216
  302.2 1.2 mul.121
  303.5 8.1 %copy.23 = f32[2,8,512,256]{3,1,2,0:T(8,128)} copy(f32[2,8,512,256]{3,2,1,0:T(8,128)S(1)} %bitcast.40) | data formatting | bytes 16777216
  311.5 14.4 %all-reduce.2.cloned.1.call-done = bf16[128,2048]{1,0:T(8,128)(2,1)} async-done(((bf16[128,2048]{1,0:T(8,128)(2,1)}), bf16[128,2048]{1,0:T(8,128)(2,1)}) %all-reduce.2.cloned.1.call-update) | async-done | bytes 524304 | tf_op jit(solution)/shard_map/psum | solution.py:88
  325.9 3.8 convolution_convert_fusion.3
  329.7 0.0 reduce-scatter.8.cloned.1.call-update
  329.7 0.0 copy-start.1
  329.7 12.4 %multiply_add_fusion = f32[16,131072]{1,0:T(8,128)} fusion(f32[16,131072]{1,0:T(8,128)} %bitcast.42, f32[16,131072]{1,0:T(8,128)} %bitcast.43, f32[16,131072]{1,0:T(8,128)} %param.15), kind=kLoop, calls=%fused_computation | loop fusion | flops 4194304 | bytes 33554432 | tf_op jit(solution)/shard_map/add | solution.py:62
  342.1 50.0 %reduce-scatter.8.cloned.1.call-done = bf16[16,1024]{1,0:T(8,128)(2,1)} async-done(((bf16[128,1024]{1,0:T(8,128)(2,1)}), bf16[16,1024]{1,0:T(8,128)(2,1)}) %reduce-scatter.8.cloned.1.call-update) | async-done | bytes 32784 | tf_op jit(solution)/shard_map/reduce_scatter | solution.py:91
  392.1 0.0 copy-done.1
  392.1 1.4 fusion.12
  (11 shorter events, 0.2 us)
Async XLA Ops:
  15.5 16.4 %all-to-all-start = ((bf16[16,8,512]{2,0,1:T(8,128)(2,1)}), bf16[16,8,512]{2,0,1:T(8,128)(2,1)S(1)}, u32[]{:S(2)}, u32[]{:S(2)}) async-start(bf16[16,8,512]{2,0,1:T(8,128)(2,1)} %bitcast.37), calls=%async_computation | async-start | bytes 262144 | tf_op jit(solution)/shard_map/all_to_all | solution.py:39
  21.7 79.1 %reduce-scatter.4.cloned.1.call-start = ((), (), s32[]{:S(2)}) async-start(), calls=%async_computation.4 | async-start | bytes 1032192 | tf_op jit(solution)/shard_map/reduce_scatter | solution.py:42
  35.6 191.2 %all-gather.2.cloned.1.call-start = ((), (), s32[]{:S(2)}) async-start(), calls=%async_computation.5 | async-start | bytes 9437184 | tf_op jit(solution)/shard_map/all_gather | solution.py:71
  36.4 213.7 %reduce-scatter.6.cloned.1.call-start = ((), (), s32[]{:S(2)}) async-start(), calls=%async_computation.6 | async-start | bytes 163840 | tf_op jit(solution)/shard_map/reduce_scatter | solution.py:73
  36.4 9.3 %copy-start.4 = (bf16[256]{0:T(256)(128)(2,1)S(1)}, bf16[256]{0:T(256)(128)(2,1)}, u32[]{:S(2)}) copy-start(bf16[256]{0:T(256)(128)(2,1)} %param.23) | copy-start | bytes 1540
  36.4 65.2 %copy-start.2 = (f32[512]{0:T(512)S(1)}, f32[512]{0:T(512)}, u32[]{:S(2)}) copy-start(f32[512]{0:T(512)} %param.22) | copy-start | bytes 6148
  110.8 121.4 %copy-start.3 = (bf16[1024]{0:T(1024)(128)(2,1)S(1)}, bf16[1024]{0:T(1024)(128)(2,1)}, u32[]{:S(2)}) copy-start(bf16[1024]{0:T(1024)(128)(2,1)} %param.25) | copy-start | bytes 6148
  110.8 139.3 %copy-start = (bf16[16,1024]{1,0:T(8,128)(2,1)S(1)}, bf16[16,1024]{1,0:T(8,128)(2,1)}, u32[]{:S(2)}) copy-start(bf16[16,1024]{1,0:T(8,128)(2,1)} %param.14) | copy-start | bytes 98308
  232.1 93.8 %all-reduce.2.cloned.1.call-start = ((), (), s32[]{:S(2)}) async-start(), calls=%async_computation.7 | async-start | bytes 1048576 | tf_op jit(solution)/shard_map/psum | solution.py:88
  292.5 99.6 %reduce-scatter.8.cloned.1.call-start = ((), (), s32[]{:S(2)}) async-start(), calls=%async_computation.8 | async-start | bytes 294912 | tf_op jit(solution)/shard_map/reduce_scatter | solution.py:91
  329.7 62.4 %copy-start.1 = (bf16[16,1024]{1,0:T(8,128)(2,1)S(1)}, bf16[16,1024]{1,0:T(8,128)(2,1)}, u32[]{:S(2)}) copy-start(bf16[16,1024]{1,0:T(8,128)(2,1)} %reduce-scatter.6.cloned.1.call-done) | copy-start | bytes 98308
Sparse Core Ops, SparseCore 0:
  35.8 65.0 reduce-scatter.3
  102.8 123.9 all-gather.1
  232.2 17.7 reduce-scatter.5
  292.6 33.2 all-reduce.1
  329.8 62.2 reduce-scatter.7
where the time goes:
time: 401 us; the launch traced here: 400 us
  waiting for transfers between devices  254 us (63%)
  blocking collectives  43.6 us (11%)
  local copies, waits for them, and re-layouts  37.8 us (9%)
  matrix products  24.1 us (6%)
  other arithmetic  20.2 us (5%)
  between operations  13.9 us (3%)
  starting transfers between devices  6.6 us (2%)
    all_gather x1, waiting for transfers between devices, body(): lax.all_gather(w_out, 'kv', axis=1, tiled=True)  116 us
    reduce_scatter x1, waiting for transfers between devices, body(): lax.psum_scatter(jnp.dot(block_rows, joined, preferred_element_type=jnp.f...  55.1 us
    reduce_scatter x1, waiting for transfers between devices, body(): lax.psum_scatter(jnp.dot(block_rows, w_down, preferred_element_type=jnp.f...  50 us
    unnamed x18, local copies, waits for them, and re-layouts  33.5 us
    all_gather x1, blocking collectives, body(): lax.all_gather(mlp_input, 'kv', axis=0, tiled=True)  31.1 us
    reduce_scatter x1, waiting for transfers between devices, body(): lax.psum_scatter(partial_out.astype(jnp.float32).astype(jnp.bfloat16), 't...  17.9 us
    psum x1, waiting for transfers between devices, body(): lax.psum(up_partial.astype(jnp.float32).astype(jnp.bfloat16), 'tp')  14.4 us
    add x1, other arithmetic, body(): jnp.exp(log_decay)[..., None] * carried  12.4 us
  transfers between devices with their start and end apart: 6, of which 5 were waited for; matrix products, arithmetic and copies ran while one was open for 15% of the time, Pallas kernels for 0%

commit v1 on v0

--- a/solution.py
+++ b/solution.py
@@ -68,7 +68,9 @@
     mixed = (mixed * head_gain.astype(jnp.float32) * jax.nn.silu(gate_heads)).astype(jnp.bfloat16)
     mixed = mixed.reshape(seq_rows, heads_here * DV)
     partial_out = jnp.dot(
-        mixed, lax.all_gather(w_out, "kv", axis=1, tiled=True), preferred_element_type=jnp.float32
+        mixed,
+        jnp.concatenate(lax.all_gather(w_out, "kv"), axis=1),
+        preferred_element_type=jnp.float32,
     ).astype(jnp.bfloat16)
     attn_out = lax.psum_scatter(
         partial_out.astype(jnp.float32).astype(jnp.bfloat16), "tp", scatter_dimension=1, tiled=True

time: 401 us -> 413 us (1.030)
  local copies, waits for them, and re-layouts: 37.8 us -> 49.1 us
    reshape x0 -> x1, local copies, waits for them, and re-layouts: none -> 11.4 us  [body(): jnp.concatenate(lax.all_gather(w_out, 'kv'), axis=1)]
where the time goes in v1:
time: 413 us; the launch traced here: 412 us
  waiting for transfers between devices  253 us (61%)
  local copies, waits for them, and re-layouts  49.1 us (12%)
  blocking collectives  43.6 us (11%)
  matrix products  25.2 us (6%)
  other arithmetic  20.2 us (5%)
  between operations  13.9 us (3%)
  starting transfers between devices  6.6 us (2%)
    all_gather x1, waiting for transfers between devices, body(): lax.all_gather(w_out, 'kv')  115 us
    reduce_scatter x1, waiting for transfers between devices, body(): lax.psum_scatter(jnp.dot(block_rows, joined, preferred_element_type=jnp.f...  55.1 us
    reduce_scatter x1, waiting for transfers between devices, body(): lax.psum_scatter(jnp.dot(block_rows, w_down, preferred_element_type=jnp.f...  50 us
    unnamed x18, local copies, waits for them, and re-layouts  33.5 us
    all_gather x1, blocking collectives, body(): lax.all_gather(mlp_input, 'kv', axis=0, tiled=True)  31.1 us
    reduce_scatter x1, waiting for transfers between devices, body(): lax.psum_scatter(partial_out.astype(jnp.float32).astype(jnp.bfloat16), 't...  17.9 us
    psum x1, waiting for transfers between devices, body(): lax.psum(up_partial.astype(jnp.float32).astype(jnp.bfloat16), 'tp')  14.3 us
    add x1, other arithmetic, body(): jnp.exp(log_decay)[..., None] * carried  12.4 us
  transfers between devices with their start and end apart: 6, of which 5 were waited for; matrix products, arithmetic and copies ran while one was open for 15% of the time, Pallas kernels for 0%

profile of v1, /device:TPU:0, one launch (start us, length us, event | category | flops | bytes accessed | tf_op | source)
XLA Modules:
  0.0 412.1 jit_solution(9366324042291345289)
XLA Ops:
  7.2 6.7 %all_gather.12 = bf16[16,4096]{1,0:T(8,128)(2,1)S(1)} all-gather(bf16[16,1024]{1,0:T(8,128)(2,1)} %param.14), channel_id=1, replica_groups=mesh['kv'=8,'tp'=4] {'tp'}, dimensions={1}, use_global_device_ids=true | all-gather | bytes 163840 | tf_op jit(solution)/shard_map/all_gather | solution.py:31
  13.9 0.1 fusion.5
  14.0 0.7 convert_element_type.78
  14.7 0.1 fusion.7
  14.8 0.7 copy.30
  15.5 6.2 %all-to-all-start = ((bf16[16,8,512]{2,0,1:T(8,128)(2,1)}), bf16[16,8,512]{2,0,1:T(8,128)(2,1)S(1)}, u32[]{:S(2)}, u32[]{:S(2)}) async-start(bf16[16,8,512]{2,0,1:T(8,128)(2,1)} %bitcast.41), calls=%async_computation | async-start | bytes 262144 | tf_op jit(solution)/shard_map/all_to_all | solution.py:39
  21.7 0.0 reduce-scatter.4.cloned.1.call-start
  21.8 1.9 constant_dynamic-update-slice_fusion.4
  23.6 1.9 constant_dynamic-update-slice_fusion.3
  25.5 1.9 constant_dynamic-update-slice_fusion.2
  27.4 2.3 constant_dynamic-update-slice_fusion.1
  29.6 2.3 constant_dynamic-update-slice_fusion
  31.9 0.0 all-to-all-done
  31.9 3.7 convolution_convert_fusion
  35.6 0.0 reduce-scatter.4.cloned.1.call-update
  35.6 0.0 all-gather.3.cloned.1.call-start
  35.7 0.7 all-gather.3.cloned.1.call-update
  36.4 0.0 reduce-scatter.6.cloned.1.call-start
  36.4 0.0 copy-start.4
  36.4 0.0 copy-start.2
  36.5 9.3 %copy.23 = f32[2,8,512,256]{3,2,1,0:T(8,128)} copy(f32[2,8,512,256]{3,1,2,0:T(8,128)} %bitcast.46) | data formatting | bytes 16777216
  45.7 0.0 copy-done.4
  45.7 55.1 %reduce-scatter.4.cloned.1.call-done = bf16[16,3584]{1,0:T(8,128)(2,1)} async-done(((bf16[128,3584]{1,0:T(8,128)(2,1)}), bf16[16,3584]{1,0:T(8,128)(2,1)}) %reduce-scatter.4.cloned.1.call-update) | async-done | bytes 114704 | tf_op jit(solution)/shard_map/reduce_scatter | solution.py:42
  100.8 0.8 slice_convert_fusion.1
  101.6 0.0 copy-done.2
  101.6 0.8 fusion.18
  102.5 0.7 slice_convert_fusion.2
  103.2 7.5 %fusion = f32[16,4,1,256]{3,2,1,0:T(1,128)S(1)} fusion(f32[16,4,128,1]{2,3,1,0:T(1,128)S(1)} %bitcast.52, f32[16,4,128,256]{3,2,1,0:T(8,128)} %bitcast.42, f32[16,4,128]{2,1,0:T(4,128)S(1)} %exp.21, f32[16,4,256]{2,1,0:T(4,128)S(1)} %reshape.70, f32[16,4,128]{2,1,0:T(4,128)S(1)} %reshape.69), kind=kOutput, calls=%fused_computation.1 | convolution fusion | flops 31457280 | bytes 8617984 | tf_op jit(solution)/shard_map/bhk,bhkv->bhv/dot_general | solution.py:65
  110.8 0.1 fusion.13
  110.9 0.1 fusion.15
  111.0 115.5 %all-gather.3.cloned.1.call-done = bf16[8192,512]{1,0:T(8,128)(2,1)} async-done(((bf16[1024,512]{1,0:T(8,128)(2,1)}), bf16[8192,512]{1,0:T(8,128)(2,1)}) %all-gather.3.cloned.1.call-update) | async-done | bytes 8388624 | tf_op jit(solution)/shard_map/all_gather | solution.py:72
  226.5 11.4 %copy.19 = bf16[1024,8,512]{0,2,1:T(8,128)(2,1)} copy(bf16[1024,8,512]{2,0,1:T(8,128)(2,1)} %bitcast.49) | data formatting | bytes 16777216 | tf_op jit(solution)/shard_map/reshape | solution.py:72
  237.8 0.0 copy-start.3
  237.8 0.0 copy-start
  237.8 6.3 %convolution_convert_fusion.1 = bf16[16,4096]{1,0:T(8,128)(2,1)} fusion(bf16[16,1024]{1,0:T(8,128)(2,1)S(1)} %bitcast.53, bf16[1024,4096]{0,1:T(8,128)(2,1)} %bitcast.43), kind=kOutput, calls=%fused_computation.5 | convolution fusion | flops 134283264 | bytes 8552448 | tf_op jit(solution)/shard_map/dot_general | solution.py:70
  244.1 0.0 reduce-scatter.6.cloned.1.call-update
  244.2 0.0 all-reduce.2.cloned.1.call-start
  244.2 0.0 copy-done.3
  244.2 17.9 %reduce-scatter.6.cloned.1.call-done = bf16[16,1024]{1,0:T(8,128)(2,1)} async-done(((bf16[16,4096]{1,0:T(8,128)(2,1)}), bf16[16,1024]{1,0:T(8,128)(2,1)}) %reduce-scatter.6.cloned.1.call-update) | async-done | bytes 32784 | tf_op jit(solution)/shard_map/reduce_scatter | solution.py:75
  262.2 0.0 copy-done
  262.2 0.9 fusion.9
  263.0 5.8 %psum.14 = f32[16]{0:T(128)S(1)} all-reduce(f32[16]{0:T(128)S(1)} %fusion.9), channel_id=1, replica_groups=mesh['kv'=8,'tp'=4] {'tp'}, use_global_device_ids=true, to_apply=%region_5.6 | all-reduce | flops 16 | bytes 128 | tf_op jit(solution)/shard_map/psum | solution.py:80
  268.8 0.8 fusion.11
  269.6 31.1 %all_gather.15 = bf16[128,1024]{1,0:T(8,128)(2,1)S(1)} all-gather(bf16[16,1024]{1,0:T(8,128)(2,1)S(1)} %fusion.11), channel_id=1, replica_groups=mesh['kv'=8,'tp'=4] {'kv'}, dimensions={0}, use_global_device_ids=true | all-gather | bytes 294912 | tf_op jit(solution)/shard_map/all_gather | solution.py:86
  300.8 3.8 convolution_convert_fusion.2
  304.6 0.0 all-reduce.2.cloned.1.call-update
  304.6 0.2 reduce-scatter.8.cloned.1.call-start
  304.8 1.3 broadcast_multiply_fusion
  306.1 8.3 %copy.26 = f32[2,8,512,256]{3,1,2,0:T(8,128)} copy(f32[2,8,512,256]{3,2,1,0:T(8,128)S(1)} %bitcast.44) | data formatting | bytes 16777216
  314.4 1.2 mul.121
  315.6 8.1 %copy.25 = f32[2,8,512,256]{3,1,2,0:T(8,128)} copy(f32[2,8,512,256]{3,2,1,0:T(8,128)S(1)} %bitcast.45) | data formatting | bytes 16777216
  323.7 14.3 %all-reduce.2.cloned.1.call-done = bf16[128,2048]{1,0:T(8,128)(2,1)} async-done(((bf16[128,2048]{1,0:T(8,128)(2,1)}), bf16[128,2048]{1,0:T(8,128)(2,1)}) %all-reduce.2.cloned.1.call-update) | async-done | bytes 524304 | tf_op jit(solution)/shard_map/psum | solution.py:90
  338.0 3.8 convolution_convert_fusion.3
  341.8 0.0 reduce-scatter.8.cloned.1.call-update
  341.8 0.0 copy-start.1
  341.8 12.4 %multiply_add_fusion = f32[16,131072]{1,0:T(8,128)} fusion(f32[16,131072]{1,0:T(8,128)} %bitcast.47, f32[16,131072]{1,0:T(8,128)} %bitcast.48, f32[16,131072]{1,0:T(8,128)} %param.15), kind=kLoop, calls=%fused_computation | loop fusion | flops 4194304 | bytes 33554432 | tf_op jit(solution)/shard_map/add | solution.py:62
  354.2 50.0 %reduce-scatter.8.cloned.1.call-done = bf16[16,1024]{1,0:T(8,128)(2,1)} async-done(((bf16[128,1024]{1,0:T(8,128)(2,1)}), bf16[16,1024]{1,0:T(8,128)(2,1)}) %reduce-scatter.8.cloned.1.call-update) | async-done | bytes 32784 | tf_op jit(solution)/shard_map/reduce_scatter | solution.py:93
  404.2 0.0 copy-done.1
  404.2 1.4 fusion.12
  (11 shorter events, 0.2 us)
Async XLA Ops:
  15.5 16.4 %all-to-all-start = ((bf16[16,8,512]{2,0,1:T(8,128)(2,1)}), bf16[16,8,512]{2,0,1:T(8,128)(2,1)S(1)}, u32[]{:S(2)}, u32[]{:S(2)}) async-start(bf16[16,8,512]{2,0,1:T(8,128)(2,1)} %bitcast.41), calls=%async_computation | async-start | bytes 262144 | tf_op jit(solution)/shard_map/all_to_all | solution.py:39
  21.7 79.1 %reduce-scatter.4.cloned.1.call-start = ((), (), s32[]{:S(2)}) async-start(), calls=%async_computation.4 | async-start | bytes 1032192 | tf_op jit(solution)/shard_map/reduce_scatter | solution.py:42
  35.6 190.8 %all-gather.3.cloned.1.call-start = ((), (), s32[]{:S(2)}) async-start(), calls=%async_computation.8 | async-start | bytes 9437184 | tf_op jit(solution)/shard_map/all_gather | solution.py:72
  36.4 225.8 %reduce-scatter.6.cloned.1.call-start = ((), (), s32[]{:S(2)}) async-start(), calls=%async_computation.5 | async-start | bytes 163840 | tf_op jit(solution)/shard_map/reduce_scatter | solution.py:75
  36.4 9.3 %copy-start.4 = (bf16[256]{0:T(256)(128)(2,1)S(1)}, bf16[256]{0:T(256)(128)(2,1)}, u32[]{:S(2)}) copy-start(bf16[256]{0:T(256)(128)(2,1)} %param.23) | copy-start | bytes 1540
  36.4 65.2 %copy-start.2 = (f32[512]{0:T(512)S(1)}, f32[512]{0:T(512)}, u32[]{:S(2)}) copy-start(f32[512]{0:T(512)} %param.22) | copy-start | bytes 6148
  237.8 6.4 %copy-start.3 = (bf16[1024]{0:T(1024)(128)(2,1)S(1)}, bf16[1024]{0:T(1024)(128)(2,1)}, u32[]{:S(2)}) copy-start(bf16[1024]{0:T(1024)(128)(2,1)} %param.25) | copy-start | bytes 6148
  237.8 24.3 %copy-start = (bf16[16,1024]{1,0:T(8,128)(2,1)S(1)}, bf16[16,1024]{1,0:T(8,128)(2,1)}, u32[]{:S(2)}) copy-start(bf16[16,1024]{1,0:T(8,128)(2,1)} %param.14) | copy-start | bytes 98308
  244.2 93.8 %all-reduce.2.cloned.1.call-start = ((), (), s32[]{:S(2)}) async-start(), calls=%async_computation.6 | async-start | bytes 1048576 | tf_op jit(solution)/shard_map/psum | solution.py:90
  304.6 99.6 %reduce-scatter.8.cloned.1.call-start = ((), (), s32[]{:S(2)}) async-start(), calls=%async_computation.7 | async-start | bytes 294912 | tf_op jit(solution)/shard_map/reduce_scatter | solution.py:93
  341.8 62.4 %copy-start.1 = (bf16[16,1024]{1,0:T(8,128)(2,1)S(1)}, bf16[16,1024]{1,0:T(8,128)(2,1)}, u32[]{:S(2)}) copy-start(bf16[16,1024]{1,0:T(8,128)(2,1)} %reduce-scatter.6.cloned.1.call-done) | copy-start | bytes 98308
Sparse Core Ops, SparseCore 0:
  35.8 65.0 reduce-scatter.3
  102.9 123.4 all-gather.2
  244.3 17.8 reduce-scatter.5
  304.7 33.2 all-reduce.1
  341.9 62.1 reduce-scatter.7
